TPU v7x, 32 devices: a whole 2x2x4 slice. The times are simulated.
32 devices in a mesh: sp: 8 (over z, y), tp: 4 (over x, core).
Axes of the slice: x: 2, y: 2, z: 4, core: 2. Of those that a mesh axis runs over, the one named last changes fastest.
Arguments:
- inputs: bfloat16 [8192, 2048], P(('sp', 'tp')), may hold values from -90 to 90
- in_gain: float32 [2048], replicated, may hold values from 0.1 to 1.9
- w_query: bfloat16 [2048, 1024], replicated, may hold values from -2 to 2
- w_key: bfloat16 [2048, 128], replicated, may hold values from -2 to 2
- w_value: bfloat16 [2048, 128], replicated, may hold values from -0.125 to 0.125
- query_gain: float32 [64], replicated, may hold values from 0 to 8, as said below
- key_gain: float32 [64], replicated, may hold values from 0 to 8, as said below
- decay_sums: float32 [8192, 16], P('sp', 'tp'), may hold values from -1173 to 0, as said below
- w_out: bfloat16 [1024, 2048], replicated, may hold values from -0.1875 to 0.1875
Outputs:
- result: bfloat16 [8192, 2048], P(('sp', 'tp'))
Inputs may be any that keep to these rules, and one draw needn't show every extreme that they name: `decay_sums`: along positions, each head's entries never rise. `query_gain`: every entry is positive. `key_gain`: every entry is positive.
All inputs are finite; a program needn't handle non-finite values.
Results may differ from a plain program's by a relative error of at most 0.015.
The roundings to bfloat16 on the way count: a program that leaves them out, or rounds other values in their place, can miss the bound.
Values may be sent and summed in bfloat16 or wider, within the bound.
A program may use at most 64 MiB of HBM per device.

v0:
```python
from functools import partial
import math
import jax
import jax.numpy as jnp
from jax import lax
from jax.sharding import PartitionSpec as P

epsilon = 1e-06


def rms_norm(vector, gain_vec):
    return (
        vector * lax.rsqrt(jnp.mean(vector * vector, axis=-1, keepdims=True) + epsilon) * gain_vec
    )


def attend_step(
    masked, query_rows, query_decay, query_pos, key_slice, value_slice, decay_slice, key_pos, inner
):
    peak, total, weighted = inner
    score_scale = query_rows.shape[2] ** (-0.5)
    scores = (
        jnp.einsum("thd,ud->htu", query_rows, key_slice, preferred_element_type=jnp.float32)
        * score_scale
    )
    scores = scores + query_decay[:, :, None] - decay_slice[:, None, :]
    if masked:
        visible = key_pos[None, :] <= query_pos[:, None]
        scores = jnp.where(visible[None], scores, -1e30)
    peak_new = jnp.maximum(peak, jnp.max(scores, axis=-1))
    weights_exp = jnp.exp(scores - peak_new[:, :, None])
    if masked:
        weights_exp = jnp.where(visible[None], weights_exp, 0.0)
    rescale = jnp.exp(peak - peak_new)
    total_new = total * rescale + jnp.sum(weights_exp, axis=-1)
    product = jnp.einsum(
        "htu,ud->thd",
        weights_exp.astype(jnp.bfloat16),
        value_slice,
        preferred_element_type=jnp.float32,
    )
    weighted_new = weighted * rescale.T[:, :, None] + product
    return (peak_new, total_new, weighted_new)


def keep_state(inner):
    return inner


def per_device(inputs, in_gain, w_query, w_key, w_value, query_gain, key_gain, decay_sums, w_out):
    tp_count = lax.axis_size("tp")
    sp_rank = lax.axis_index("sp")
    heads_dev = decay_sums.shape[1]
    head_size = query_gain.shape[0]
    kv_heads = w_key.shape[1] // head_size
    width_dev = heads_dev * head_size
    normed = rms_norm(inputs.astype(jnp.float32), in_gain).astype(jnp.bfloat16)
    row_count = normed.shape[0]
    all_heads = w_query.shape[1] // head_size
    query_all = rms_norm(
        jnp.dot(normed, w_query, preferred_element_type=jnp.float32).reshape(
            row_count, all_heads, head_size
        ),
        query_gain,
    ).astype(jnp.bfloat16)
    key_all = rms_norm(
        jnp.dot(normed, w_key, preferred_element_type=jnp.float32).reshape(
            row_count, kv_heads, head_size
        ),
        key_gain,
    ).astype(jnp.bfloat16)
    value_all = (
        jnp.dot(normed, w_value, preferred_element_type=jnp.float32)
        .astype(jnp.bfloat16)
        .reshape(row_count, kv_heads, head_size)
    )
    pair_all = jnp.repeat(
        jnp.concatenate([key_all, value_all], axis=2), tp_count // kv_heads, axis=1
    )
    packed = jnp.concatenate([query_all.reshape(row_count, tp_count, width_dev), pair_all], axis=2)
    received = lax.all_to_all(packed, "tp", split_axis=1, concat_axis=0, tiled=True)[:, 0]
    tok_rows = received.shape[0]
    queries = received[:, :width_dev].reshape(tok_rows, heads_dev, head_size)
    key_values = received[:, width_dev:]
    all_decays = lax.all_gather(decay_sums, "sp", axis=0, tiled=True)
    groups = (queries, sp_rank * tok_rows)
    prepared = []
    query_rows, first_pos = groups
    rows = query_rows.shape[0]
    query_decay = lax.dynamic_slice_in_dim(all_decays, first_pos, rows, 0).T
    query_pos = first_pos + jnp.arange(rows, dtype=jnp.int32)
    prepared.append((query_rows, query_decay, query_pos, first_pos, first_pos + rows - 1))
    initial = tuple(
        (
            (
                jnp.full((heads_dev, entry[0].shape[0]), -1e30, jnp.float32),
                jnp.zeros((heads_dev, entry[0].shape[0]), jnp.float32),
                jnp.zeros((entry[0].shape[0], heads_dev, head_size), jnp.float32),
            )
            for entry in prepared
        )
    )
    state = initial
    pieces = lax.all_gather(key_values, "sp", axis=0, tiled=True)
    piece_rows = pieces.shape[0]
    key_block = math.gcd(piece_rows, 512)

    def one_block(carry, block_index):
        key_start = block_index * key_block
        pair_slice = lax.dynamic_slice_in_dim(pieces, block_index * key_block, key_block, 0)
        key_slice = pair_slice[:, :head_size]
        value_slice = pair_slice[:, head_size:]
        decay_slice = lax.dynamic_slice_in_dim(all_decays, key_start, key_block, 0).T
        key_pos = key_start + jnp.arange(key_block, dtype=jnp.int32)
        updated = []
        for (query_rows, query_decay, query_pos, first_pos, last_pos), inner in zip(
            prepared, carry
        ):
            branch = jnp.where(
                key_start > last_pos, 0, jnp.where(key_start + key_block - 1 <= first_pos, 1, 2)
            )
            full_step = partial(
                attend_step,
                False,
                query_rows,
                query_decay,
                query_pos,
                key_slice,
                value_slice,
                decay_slice,
                key_pos,
            )
            masked_step = partial(
                attend_step,
                True,
                query_rows,
                query_decay,
                query_pos,
                key_slice,
                value_slice,
                decay_slice,
                key_pos,
            )
            updated.append(lax.switch(branch, [keep_state, full_step, masked_step], inner))
        return (tuple(updated), None)

    state, unused = lax.scan(one_block, state, jnp.arange(piece_rows // key_block, dtype=jnp.int32))
    outputs = [
        (weighted / total.T[:, :, None]).astype(jnp.bfloat16) for peak, total, weighted in state
    ]
    attended = outputs[0].reshape(tok_rows, width_dev)
    out_rows = lax.all_to_all(attended, "tp", split_axis=0, concat_axis=1, tiled=True)
    result = jnp.dot(out_rows, w_out, preferred_element_type=jnp.float32).astype(jnp.bfloat16)
    return result


def solution(mesh):
    placed = (P(("sp", "tp"), None), P(), P(), P(), P(), P(), P(), P("sp", "tp"), P())
    return jax.shard_map(
        per_device, mesh=mesh, in_specs=placed, out_specs=P(("sp", "tp"), None), check_vma=False
    )
```

profile of v0, /device:TPU:28, one launch (start us, length us, event | category | flops | bytes accessed | tf_op | source)
XLA Modules:
  0.0 254.3 jit_solution(247003745765237062)
XLA Ops:
  11.9 4.8 %fusion.51 = (f32[256,1024]{1,0:T(8,128)}, f32[256,1024]{1,0:T(8,128)S(1)}) fusion(bf16[2048,1024]{1,0:T(8,128)(2,1)} %param.16, bf16[256,2048]{1,0:T(8,128)(2,1)} %param.14, f32[2048]{0:T(1024)} %param.15, f32[256]{0:T(256)S(1)} %add_rsqrt_fusion.2), kind=kOutput, calls=%fused_computation.65 | convolution fusion | flops 1076101120 | bytes 7349248 | tf_op jit(solution)/shard_map/dot_general | solution.py:61
  19.3 14.2 %all_to_all.34 = bf16[256,4,384]{0,2,1:T(8,128)(2,1)S(1)} all-to-all(bf16[256,4,384]{0,2,1:T(8,128)(2,1)S(1)} %pad_maximum_fusion), channel_id=1, replica_groups=mesh['sp'=8,'tp'=4] {'tp'}, dimensions={1} | all-to-all | bytes 1572864 | tf_op jit(solution)/shard_map/all_to_all | solution.py:81
  34.6 31.2 %all_gather.7 = f32[8192,4]{0,1:T(4,128)S(1)} all-gather(f32[1024,4]{0,1:T(4,128)S(1)} %copy-done.1), channel_id=1, replica_groups=mesh['sp'=8,'tp'=4] {'sp'}, dimensions={0}, use_global_device_ids=true | all-gather | bytes 147456 | tf_op jit(solution)/shard_map/all_gather | solution.py:85
  66.1 15.7 %all-gather.2.cloned.1.call-done = bf16[8192,128]{1,0:T(8,128)(2,1)} async-done(((bf16[1024,128]{1,0:T(8,128)(2,1)}), bf16[8192,128]{1,0:T(8,128)(2,1)}) %all-gather.2.cloned.1.call-update) | async-done | bytes 2097168 | tf_op jit(solution)/shard_map/all_gather | solution.py:104
  81.9 149.1 %while.20 = (s32[]{:T(128)}, f32[4,1024]{1,0:T(4,128)S(1)}, f32[4,1024]{1,0:T(4,128)S(1)}, f32[1024,4,64]{0,2,1:T(8,128)S(1)}, s32[16]{0:T(128)S(1)}, /*index=5*...) while((s32[]{:T(128)}, f32[4,1024]{1,0:T(4,128)S(1)}, ...), condition=%wide.region_11.12_spmd.clone.clone, body=%wide.region_3.11_spmd.clone.clone.sunk | while | flops 577779200 | bytes 30917152 | solution.py:147
  84.5 6.3 %conditional.4 = ((f32[4,1024]{1,0:T(4,128)S(1)}, f32[4,1024]{1,0:T(4,128)S(1)}, f32[1024,4,64]{0,2,1:T(8,128)S(1)})) conditional(s32[]{:T(128)} %clamp.12, (f32[4,1024]{1,0:T(4,128)S(1)}, f32[4,1024]{1,0:T(4,128)S(1)}, f32[1024,4,64]{0,2,1:T(8,128)S(1)}) %tuple.72, (bf16[512,64]{0,1:T(8,128)(2,1)S(1)}, ...), branch_computations={%region_4.4_spmd, %region_5.7_spmd, %region_8.10_spmd} | conditional | flops 577779200 | bytes 30369832 | solution.py:144
  86.1 2.6 %fusion.11 = f32[1024,4,64]{0,2,1:T(8,128)S(1)} fusion(f32[512,1024,4]{1,0,2:T(8,128)S(1)} %get-tuple-element.449, f32[4,1024]{1,0:T(4,128)S(1)} %get-tuple-element.538, f32[4,512]{1,0:T(4,128)S(1)} %get-tuple-element.292, f32[4,1024]{1,0:T(4,128)S(1)} %get-tuple-element.291, f32[1024,4,64]{0,2,1:T(8,128)S(1)} %get-tuple-element.294, ...), kind=kOutput, calls=%fused_computation.9 | convolution fusion | flops 279445504 | bytes 10608640 | tf_op jit(solution)/shard_map/while/body/eval_jaxpr/cond/branch_1_fun/htu,ud->thd/dot_general | solution.py:36
  93.5 6.3 %conditional.4 = ((f32[4,1024]{1,0:T(4,128)S(1)}, f32[4,1024]{1,0:T(4,128)S(1)}, f32[1024,4,64]{0,2,1:T(8,128)S(1)})) conditional(s32[]{:T(128)} %clamp.12, (f32[4,1024]{1,0:T(4,128)S(1)}, f32[4,1024]{1,0:T(4,128)S(1)}, f32[1024,4,64]{0,2,1:T(8,128)S(1)}) %tuple.72, (bf16[512,64]{0,1:T(8,128)(2,1)S(1)}, ...), branch_computations={%region_4.4_spmd, %region_5.7_spmd, %region_8.10_spmd} | conditional | flops 577779200 | bytes 30369832 | solution.py:144
  95.1 2.6 %fusion.11 = f32[1024,4,64]{0,2,1:T(8,128)S(1)} fusion(f32[512,1024,4]{1,0,2:T(8,128)S(1)} %get-tuple-element.449, f32[4,1024]{1,0:T(4,128)S(1)} %get-tuple-element.538, f32[4,512]{1,0:T(4,128)S(1)} %get-tuple-element.292, f32[4,1024]{1,0:T(4,128)S(1)} %get-tuple-element.291, f32[1024,4,64]{0,2,1:T(8,128)S(1)} %get-tuple-element.294, ...), kind=kOutput, calls=%fused_computation.9 | convolution fusion | flops 279445504 | bytes 10608640 | tf_op jit(solution)/shard_map/while/body/eval_jaxpr/cond/branch_1_fun/htu,ud->thd/dot_general | solution.py:36
  102.5 6.3 %conditional.4 = ((f32[4,1024]{1,0:T(4,128)S(1)}, f32[4,1024]{1,0:T(4,128)S(1)}, f32[1024,4,64]{0,2,1:T(8,128)S(1)})) conditional(s32[]{:T(128)} %clamp.12, (f32[4,1024]{1,0:T(4,128)S(1)}, f32[4,1024]{1,0:T(4,128)S(1)}, f32[1024,4,64]{0,2,1:T(8,128)S(1)}) %tuple.72, (bf16[512,64]{0,1:T(8,128)(2,1)S(1)}, ...), branch_computations={%region_4.4_spmd, %region_5.7_spmd, %region_8.10_spmd} | conditional | flops 577779200 | bytes 30369832 | solution.py:144
  104.1 2.6 %fusion.11 = f32[1024,4,64]{0,2,1:T(8,128)S(1)} fusion(f32[512,1024,4]{1,0,2:T(8,128)S(1)} %get-tuple-element.449, f32[4,1024]{1,0:T(4,128)S(1)} %get-tuple-element.538, f32[4,512]{1,0:T(4,128)S(1)} %get-tuple-element.292, f32[4,1024]{1,0:T(4,128)S(1)} %get-tuple-element.291, f32[1024,4,64]{0,2,1:T(8,128)S(1)} %get-tuple-element.294, ...), kind=kOutput, calls=%fused_computation.9 | convolution fusion | flops 279445504 | bytes 10608640 | tf_op jit(solution)/shard_map/while/body/eval_jaxpr/cond/branch_1_fun/htu,ud->thd/dot_general | solution.py:36
  111.5 6.3 %conditional.4 = ((f32[4,1024]{1,0:T(4,128)S(1)}, f32[4,1024]{1,0:T(4,128)S(1)}, f32[1024,4,64]{0,2,1:T(8,128)S(1)})) conditional(s32[]{:T(128)} %clamp.12, (f32[4,1024]{1,0:T(4,128)S(1)}, f32[4,1024]{1,0:T(4,128)S(1)}, f32[1024,4,64]{0,2,1:T(8,128)S(1)}) %tuple.72, (bf16[512,64]{0,1:T(8,128)(2,1)S(1)}, ...), branch_computations={%region_4.4_spmd, %region_5.7_spmd, %region_8.10_spmd} | conditional | flops 577779200 | bytes 30369832 | solution.py:144
  120.4 6.3 %conditional.4 = ((f32[4,1024]{1,0:T(4,128)S(1)}, f32[4,1024]{1,0:T(4,128)S(1)}, f32[1024,4,64]{0,2,1:T(8,128)S(1)})) conditional(s32[]{:T(128)} %clamp.12, (f32[4,1024]{1,0:T(4,128)S(1)}, f32[4,1024]{1,0:T(4,128)S(1)}, f32[1024,4,64]{0,2,1:T(8,128)S(1)}) %tuple.72, (bf16[512,64]{0,1:T(8,128)(2,1)S(1)}, ...), branch_computations={%region_4.4_spmd, %region_5.7_spmd, %region_8.10_spmd} | conditional | flops 577779200 | bytes 30369832 | solution.py:144
  122.0 2.6 %fusion.11 = f32[1024,4,64]{0,2,1:T(8,128)S(1)} fusion(f32[512,1024,4]{1,0,2:T(8,128)S(1)} %get-tuple-element.449, f32[4,1024]{1,0:T(4,128)S(1)} %get-tuple-element.538, f32[4,512]{1,0:T(4,128)S(1)} %get-tuple-element.292, f32[4,1024]{1,0:T(4,128)S(1)} %get-tuple-element.291, f32[1024,4,64]{0,2,1:T(8,128)S(1)} %get-tuple-element.294, ...), kind=kOutput, calls=%fused_computation.9 | convolution fusion | flops 279445504 | bytes 10608640 | tf_op jit(solution)/shard_map/while/body/eval_jaxpr/cond/branch_1_fun/htu,ud->thd/dot_general | solution.py:36
  129.4 6.3 %conditional.4 = ((f32[4,1024]{1,0:T(4,128)S(1)}, f32[4,1024]{1,0:T(4,128)S(1)}, f32[1024,4,64]{0,2,1:T(8,128)S(1)})) conditional(s32[]{:T(128)} %clamp.12, (f32[4,1024]{1,0:T(4,128)S(1)}, f32[4,1024]{1,0:T(4,128)S(1)}, f32[1024,4,64]{0,2,1:T(8,128)S(1)}) %tuple.72, (bf16[512,64]{0,1:T(8,128)(2,1)S(1)}, ...), branch_computations={%region_4.4_spmd, %region_5.7_spmd, %region_8.10_spmd} | conditional | flops 577779200 | bytes 30369832 | solution.py:144
  131.0 2.6 %fusion.11 = f32[1024,4,64]{0,2,1:T(8,128)S(1)} fusion(f32[512,1024,4]{1,0,2:T(8,128)S(1)} %get-tuple-element.449, f32[4,1024]{1,0:T(4,128)S(1)} %get-tuple-element.538, f32[4,512]{1,0:T(4,128)S(1)} %get-tuple-element.292, f32[4,1024]{1,0:T(4,128)S(1)} %get-tuple-element.291, f32[1024,4,64]{0,2,1:T(8,128)S(1)} %get-tuple-element.294, ...), kind=kOutput, calls=%fused_computation.9 | convolution fusion | flops 279445504 | bytes 10608640 | tf_op jit(solution)/shard_map/while/body/eval_jaxpr/cond/branch_1_fun/htu,ud->thd/dot_general | solution.py:36
  138.4 6.3 %conditional.4 = ((f32[4,1024]{1,0:T(4,128)S(1)}, f32[4,1024]{1,0:T(4,128)S(1)}, f32[1024,4,64]{0,2,1:T(8,128)S(1)})) conditional(s32[]{:T(128)} %clamp.12, (f32[4,1024]{1,0:T(4,128)S(1)}, f32[4,1024]{1,0:T(4,128)S(1)}, f32[1024,4,64]{0,2,1:T(8,128)S(1)}) %tuple.72, (bf16[512,64]{0,1:T(8,128)(2,1)S(1)}, ...), branch_computations={%region_4.4_spmd, %region_5.7_spmd, %region_8.10_spmd} | conditional | flops 577779200 | bytes 30369832 | solution.py:144
  147.4 6.3 %conditional.4 = ((f32[4,1024]{1,0:T(4,128)S(1)}, f32[4,1024]{1,0:T(4,128)S(1)}, f32[1024,4,64]{0,2,1:T(8,128)S(1)})) conditional(s32[]{:T(128)} %clamp.12, (f32[4,1024]{1,0:T(4,128)S(1)}, f32[4,1024]{1,0:T(4,128)S(1)}, f32[1024,4,64]{0,2,1:T(8,128)S(1)}) %tuple.72, (bf16[512,64]{0,1:T(8,128)(2,1)S(1)}, ...), branch_computations={%region_4.4_spmd, %region_5.7_spmd, %region_8.10_spmd} | conditional | flops 577779200 | bytes 30369832 | solution.py:144
  156.3 6.3 %conditional.4 = ((f32[4,1024]{1,0:T(4,128)S(1)}, f32[4,1024]{1,0:T(4,128)S(1)}, f32[1024,4,64]{0,2,1:T(8,128)S(1)})) conditional(s32[]{:T(128)} %clamp.12, (f32[4,1024]{1,0:T(4,128)S(1)}, f32[4,1024]{1,0:T(4,128)S(1)}, f32[1024,4,64]{0,2,1:T(8,128)S(1)}) %tuple.72, (bf16[512,64]{0,1:T(8,128)(2,1)S(1)}, ...), branch_computations={%region_4.4_spmd, %region_5.7_spmd, %region_8.10_spmd} | conditional | flops 577779200 | bytes 30369832 | solution.py:144
  165.3 6.3 %conditional.4 = ((f32[4,1024]{1,0:T(4,128)S(1)}, f32[4,1024]{1,0:T(4,128)S(1)}, f32[1024,4,64]{0,2,1:T(8,128)S(1)})) conditional(s32[]{:T(128)} %clamp.12, (f32[4,1024]{1,0:T(4,128)S(1)}, f32[4,1024]{1,0:T(4,128)S(1)}, f32[1024,4,64]{0,2,1:T(8,128)S(1)}) %tuple.72, (bf16[512,64]{0,1:T(8,128)(2,1)S(1)}, ...), branch_computations={%region_4.4_spmd, %region_5.7_spmd, %region_8.10_spmd} | conditional | flops 577779200 | bytes 30369832 | solution.py:144
  174.3 6.3 %conditional.4 = ((f32[4,1024]{1,0:T(4,128)S(1)}, f32[4,1024]{1,0:T(4,128)S(1)}, f32[1024,4,64]{0,2,1:T(8,128)S(1)})) conditional(s32[]{:T(128)} %clamp.12, (f32[4,1024]{1,0:T(4,128)S(1)}, f32[4,1024]{1,0:T(4,128)S(1)}, f32[1024,4,64]{0,2,1:T(8,128)S(1)}) %tuple.72, (bf16[512,64]{0,1:T(8,128)(2,1)S(1)}, ...), branch_computations={%region_4.4_spmd, %region_5.7_spmd, %region_8.10_spmd} | conditional | flops 577779200 | bytes 30369832 | solution.py:144
  183.3 6.3 %conditional.4 = ((f32[4,1024]{1,0:T(4,128)S(1)}, f32[4,1024]{1,0:T(4,128)S(1)}, f32[1024,4,64]{0,2,1:T(8,128)S(1)})) conditional(s32[]{:T(128)} %clamp.12, (f32[4,1024]{1,0:T(4,128)S(1)}, f32[4,1024]{1,0:T(4,128)S(1)}, f32[1024,4,64]{0,2,1:T(8,128)S(1)}) %tuple.72, (bf16[512,64]{0,1:T(8,128)(2,1)S(1)}, ...), branch_computations={%region_4.4_spmd, %region_5.7_spmd, %region_8.10_spmd} | conditional | flops 577779200 | bytes 30369832 | solution.py:144
  192.3 6.3 %conditional.4 = ((f32[4,1024]{1,0:T(4,128)S(1)}, f32[4,1024]{1,0:T(4,128)S(1)}, f32[1024,4,64]{0,2,1:T(8,128)S(1)})) conditional(s32[]{:T(128)} %clamp.12, (f32[4,1024]{1,0:T(4,128)S(1)}, f32[4,1024]{1,0:T(4,128)S(1)}, f32[1024,4,64]{0,2,1:T(8,128)S(1)}) %tuple.72, (bf16[512,64]{0,1:T(8,128)(2,1)S(1)}, ...), branch_computations={%region_4.4_spmd, %region_5.7_spmd, %region_8.10_spmd} | conditional | flops 577779200 | bytes 30369832 | solution.py:144
  201.2 6.3 %conditional.4 = ((f32[4,1024]{1,0:T(4,128)S(1)}, f32[4,1024]{1,0:T(4,128)S(1)}, f32[1024,4,64]{0,2,1:T(8,128)S(1)})) conditional(s32[]{:T(128)} %clamp.12, (f32[4,1024]{1,0:T(4,128)S(1)}, f32[4,1024]{1,0:T(4,128)S(1)}, f32[1024,4,64]{0,2,1:T(8,128)S(1)}) %tuple.72, (bf16[512,64]{0,1:T(8,128)(2,1)S(1)}, ...), branch_computations={%region_4.4_spmd, %region_5.7_spmd, %region_8.10_spmd} | conditional | flops 577779200 | bytes 30369832 | solution.py:144
  210.2 9.1 %conditional.4 = ((f32[4,1024]{1,0:T(4,128)S(1)}, f32[4,1024]{1,0:T(4,128)S(1)}, f32[1024,4,64]{0,2,1:T(8,128)S(1)})) conditional(s32[]{:T(128)} %clamp.12, (f32[4,1024]{1,0:T(4,128)S(1)}, f32[4,1024]{1,0:T(4,128)S(1)}, f32[1024,4,64]{0,2,1:T(8,128)S(1)}) %tuple.72, (bf16[512,64]{0,1:T(8,128)(2,1)S(1)}, ...), branch_computations={%region_4.4_spmd, %region_5.7_spmd, %region_8.10_spmd} | conditional | flops 577779200 | bytes 30369832 | solution.py:144
  213.0 3.2 %fusion.30 = f32[1024,4,64]{0,2,1:T(8,128)S(1)} fusion(f32[512,1024,4]{1,0,2:T(8,128)S(1)} %get-tuple-element.451, f32[4,1024]{1,0:T(4,128)S(1)} %get-tuple-element.541, f32[4,512]{1,0:T(4,128)S(1)} %get-tuple-element.303, f32[4,1024]{1,0:T(4,128)S(1)} %get-tuple-element.302, pred[1024,512]{0,1:T(8,128)(4,1)S(1)} %broadcast_compare_fusion, ...), kind=kOutput, calls=%fused_computation.27 | convolution fusion | flops 283639808 | bytes 11132928 | tf_op jit(solution)/shard_map/while/body/eval_jaxpr/cond/branch_2_fun/htu,ud->thd/dot_general | solution.py:36
  216.2 3.1 %fusion.22 = f32[4,1024]{1,0:T(4,128)S(1)} fusion(f32[512,1024,4]{1,0,2:T(8,128)S(1)} %get-tuple-element.451, f32[4,1024]{1,0:T(4,128)S(1)} %get-tuple-element.541, f32[4,512]{1,0:T(4,128)S(1)} %get-tuple-element.303, f32[4,1024]{1,0:T(4,128)S(1)} %get-tuple-element.302, pred[1024,512]{0,1:T(8,128)(4,1)S(1)} %broadcast_compare_fusion), kind=kLoop, calls=%fused_computation.22 | loop fusion | flops 14675968 | bytes 8970240 | tf_op jit(solution)/shard_map/while/body/eval_jaxpr/cond/branch_2_fun/reduce_sum | solution.py:35
  221.9 9.1 %conditional.4 = ((f32[4,1024]{1,0:T(4,128)S(1)}, f32[4,1024]{1,0:T(4,128)S(1)}, f32[1024,4,64]{0,2,1:T(8,128)S(1)})) conditional(s32[]{:T(128)} %clamp.12, (f32[4,1024]{1,0:T(4,128)S(1)}, f32[4,1024]{1,0:T(4,128)S(1)}, f32[1024,4,64]{0,2,1:T(8,128)S(1)}) %tuple.72, (bf16[512,64]{0,1:T(8,128)(2,1)S(1)}, ...), branch_computations={%region_4.4_spmd, %region_5.7_spmd, %region_8.10_spmd} | conditional | flops 577779200 | bytes 30369832 | solution.py:144
  224.7 3.2 %fusion.30 = f32[1024,4,64]{0,2,1:T(8,128)S(1)} fusion(f32[512,1024,4]{1,0,2:T(8,128)S(1)} %get-tuple-element.451, f32[4,1024]{1,0:T(4,128)S(1)} %get-tuple-element.541, f32[4,512]{1,0:T(4,128)S(1)} %get-tuple-element.303, f32[4,1024]{1,0:T(4,128)S(1)} %get-tuple-element.302, pred[1024,512]{0,1:T(8,128)(4,1)S(1)} %broadcast_compare_fusion, ...), kind=kOutput, calls=%fused_computation.27 | convolution fusion | flops 283639808 | bytes 11132928 | tf_op jit(solution)/shard_map/while/body/eval_jaxpr/cond/branch_2_fun/htu,ud->thd/dot_general | solution.py:36
  227.9 3.1 %fusion.22 = f32[4,1024]{1,0:T(4,128)S(1)} fusion(f32[512,1024,4]{1,0,2:T(8,128)S(1)} %get-tuple-element.451, f32[4,1024]{1,0:T(4,128)S(1)} %get-tuple-element.541, f32[4,512]{1,0:T(4,128)S(1)} %get-tuple-element.303, f32[4,1024]{1,0:T(4,128)S(1)} %get-tuple-element.302, pred[1024,512]{0,1:T(8,128)(4,1)S(1)} %broadcast_compare_fusion), kind=kLoop, calls=%fused_computation.22 | loop fusion | flops 14675968 | bytes 8970240 | tf_op jit(solution)/shard_map/while/body/eval_jaxpr/cond/branch_2_fun/reduce_sum | solution.py:35
  231.6 11.5 %all_to_all.35 = bf16[4,256,256]{1,2,0:T(8,128)(2,1)S(1)} all-to-all(bf16[4,256,256]{1,2,0:T(8,128)(2,1)S(1)} %copy.41), channel_id=1, replica_groups=mesh['sp'=8,'tp'=4] {'tp'}, dimensions={0} | all-to-all | bytes 1048576 | tf_op jit(solution)/shard_map/all_to_all | solution.py:152
  243.1 4.4 %convolution_convert_fusion = bf16[256,2048]{1,0:T(8,128)(2,1)} fusion(bf16[256,1024]{0,1:T(8,128)(2,1)S(1)} %bitcast.110, bf16[1024,2048]{1,0:T(8,128)(2,1)} %param.22), kind=kOutput, calls=%fused_computation.44 | convolution fusion | flops 1074266112 | bytes 5767168 | tf_op jit(solution)/shard_map/dot_general | solution.py:153
  (244 shorter events, 120.4 us)
Async XLA Ops:
  6.5 1.6 copy-start
  6.5 75.2 %all-gather.2.cloned.1.call-start = ((), (), s32[]{:S(2)}) async-start(), calls=%async_computation.2 | async-start | bytes 2359296 | tf_op jit(solution)/shard_map/all_gather | solution.py:104
  8.1 10.6 %copy-start.3 = (f32[64]{0:T(128)S(1)}, f32[64]{0:T(128)}, u32[]{:S(2)}) copy-start(f32[64]{0:T(128)} %param.19) | copy-start | bytes 772
  8.1 10.7 %copy-start.2 = (f32[64]{0:T(128)S(1)}, f32[64]{0:T(128)}, u32[]{:S(2)}) copy-start(f32[64]{0:T(128)} %param.20) | copy-start | bytes 772
  16.7 17.9 %copy-start.1 = (f32[1024,4]{0,1:T(4,128)S(1)}, f32[1024,4]{0,1:T(4,128)}, u32[]{:S(2)}) copy-start(f32[1024,4]{0,1:T(4,128)} %param.21) | copy-start | bytes 49156
Sparse Core Ops, SparseCore 0:
  34.7 46.9 all-gather.1
where the time goes:
time: 255 us; the launch traced here: 254 us
  matrix products  82.4 us (32%)
  blocking collectives  56.9 us (22%)
  other arithmetic  38.4 us (15%)
  local copies, waits for them, and re-layouts  34.4 us (13%)
  waiting for transfers between devices  15.7 us (6%)
  between operations  13.6 us (5%)
  loops' own time  13 us (5%)
    dot_general x16, matrix products, attend_step(): jnp.einsum('htu,ud->thd', weights_exp.astype(jnp.bfloat16), value_slice,...  42.9 us
    reduce_sum x16, other arithmetic, attend_step(): total_new = total * rescale + jnp.sum(weights_exp, axis=-1)  35 us
    all_gather x1, blocking collectives, per_device(): all_decays = lax.all_gather(decay_sums, 'sp', axis=0, tiled=True)  31.2 us
    dot_general x16, matrix products, attend_step(): jnp.einsum('thd,ud->htu', query_rows, key_slice, preferred_element_type=j...  26.4 us
    slice x16, local copies, waits for them, and re-layouts, one_block(): value_slice = pair_slice[:, head_size:]  17.6 us
    all_gather x1, waiting for transfers between devices, per_device(): pieces = lax.all_gather(key_values, 'sp', axis=0, tiled=True)  15.7 us
    all_to_all x1, blocking collectives, per_device(): lax.all_to_all(packed, 'tp', split_axis=1, concat_axis=0, tiled=True)[:, 0]  14.2 us
    another operation x1, loops' own time, per_device(): lax.scan(one_block, state, jnp.arange(piece_rows // key_block, dtype=jnp....  11.8 us
  transfers between devices with their start and end apart: 1, of which 1 were waited for; matrix products, arithmetic and copies ran while one was open for 0% of the time, Pallas kernels for 0%

commit v1 on v0

--- a/solution.py
+++ b/solution.py
@@ -1,3 +1,4 @@
+import functools
 from functools import partial
 import math
 import jax
@@ -6,6 +7,19 @@
 from jax.sharding import PartitionSpec as P
 
 epsilon = 1e-06
+
+
+def cycles_scan(t0, d_out, where_dim):
+    side_arr = lax.all_to_all(
+        jnp.stack(jnp.split(t0, lax.axis_size("tp"), d_out)),
+        axis_name="tp",
+        split_axis=0,
+        concat_axis=0,
+    )
+    return jnp.concatenate(side_arr, axis=where_dim)
+
+
+carry_knots = functools.partial(cycles_scan, d_out=1, where_dim=0)
 
 
 def rms_norm(vector, gain_vec):
@@ -78,7 +92,7 @@
         jnp.concatenate([key_all, value_all], axis=2), tp_count // kv_heads, axis=1
     )
     packed = jnp.concatenate([query_all.reshape(row_count, tp_count, width_dev), pair_all], axis=2)
-    received = lax.all_to_all(packed, "tp", split_axis=1, concat_axis=0, tiled=True)[:, 0]
+    received = carry_knots(packed)[:, 0]
     tok_rows = received.shape[0]
     queries = received[:, :width_dev].reshape(tok_rows, heads_dev, head_size)
     key_values = received[:, width_dev:]

time: 255 us -> 257 us (level)
  no operation moved by 1% of the time
where the time goes in v1:
time: 257 us; the launch traced here: 256 us
  matrix products  83.8 us (33%)
  blocking collectives  56.8 us (22%)
  other arithmetic  39.2 us (15%)
  local copies, waits for them, and re-layouts  34.4 us (13%)
  waiting for transfers between devices  15.7 us (6%)
  between operations  13.6 us (5%)
  loops' own time  13 us (5%)
    dot_general x16, matrix products, attend_step(): jnp.einsum('htu,ud->thd', weights_exp.astype(jnp.bfloat16), value_slice,...  44 us
    reduce_sum x16, other arithmetic, attend_step(): total_new = total * rescale + jnp.sum(weights_exp, axis=-1)  35.6 us
    all_gather x1, blocking collectives, per_device(): all_decays = lax.all_gather(decay_sums, 'sp', axis=0, tiled=True)  31.2 us
    dot_general x16, matrix products, attend_step(): jnp.einsum('thd,ud->htu', query_rows, key_slice, preferred_element_type=j...  26.8 us
    slice x16, local copies, waits for them, and re-layouts, one_block(): value_slice = pair_slice[:, head_size:]  17.6 us
    all_gather x1, waiting for transfers between devices, per_device(): pieces = lax.all_gather(key_values, 'sp', axis=0, tiled=True)  15.6 us
    all_to_all x1, blocking collectives, cycles_scan(): lax.all_to_all(jnp.stack(jnp.split(t0, lax.axis_size('tp'), d_out)), axis...  14.2 us
    another operation x1, loops' own time, per_device(): lax.scan(one_block, state, jnp.arange(piece_rows // key_block, dtype=jnp....  11.8 us
  transfers between devices with their start and end apart: 1, of which 1 were waited for; matrix products, arithmetic and copies ran while one was open for 0% of the time, Pallas kernels for 0%

profile of v1, /device:TPU:28, one launch (start us, length us, event | category | flops | bytes accessed | tf_op | source)
XLA Modules:
  0.0 256.4 jit_solution(733963940798986127)
XLA Ops:
  11.9 4.8 %fusion.58 = (f32[256,1024]{1,0:T(8,128)}, f32[256,1024]{1,0:T(8,128)S(1)}) fusion(bf16[2048,1024]{1,0:T(8,128)(2,1)} %param.16, bf16[256,2048]{1,0:T(8,128)(2,1)} %param.14, f32[2048]{0:T(1024)} %param.15, f32[256]{0:T(256)S(1)} %add_rsqrt_fusion.2), kind=kOutput, calls=%fused_computation.79 | convolution fusion | flops 1076101120 | bytes 7349248 | tf_op jit(solution)/shard_map/dot_general | solution.py:75
  19.5 14.2 %all_to_all.24 = bf16[4,256,1,384]{1,3,2,0:T(8,128)(2,1)S(1)} all-to-all(bf16[4,256,1,384]{1,3,2,0:T(8,128)(2,1)S(1)} %pad_maximum_fusion), channel_id=1, replica_groups=mesh['sp'=8,'tp'=4] {'tp'}, dimensions={0} | all-to-all | bytes 1572864 | tf_op jit(solution)/shard_map/all_to_all | solution.py:13
  34.8 31.2 %all_gather.7 = f32[8192,4]{0,1:T(4,128)S(1)} all-gather(f32[1024,4]{0,1:T(4,128)S(1)} %copy-done.1), channel_id=1, replica_groups=mesh['sp'=8,'tp'=4] {'sp'}, dimensions={0}, use_global_device_ids=true | all-gather | bytes 147456 | tf_op jit(solution)/shard_map/all_gather | solution.py:99
  66.3 15.6 %all-gather.2.cloned.1.call-done = bf16[8192,128]{1,0:T(8,128)(2,1)} async-done(((bf16[1024,128]{1,0:T(8,128)(2,1)}), bf16[8192,128]{1,0:T(8,128)(2,1)}) %all-gather.2.cloned.1.call-update) | async-done | bytes 2097168 | tf_op jit(solution)/shard_map/all_gather | solution.py:118
  82.0 151.1 %while.20 = (s32[]{:T(128)}, f32[4,1024]{1,0:T(4,128)S(1)}, f32[4,1024]{1,0:T(4,128)S(1)}, f32[1024,4,64]{0,2,1:T(8,128)S(1)}, s32[16]{0:T(128)S(1)}, /*index=5*...) while((s32[]{:T(128)}, f32[4,1024]{1,0:T(4,128)S(1)}, ...), condition=%wide.region_11.12_spmd.clone.clone, body=%wide.region_3.11_spmd.clone.clone.sunk | while | flops 577779200 | bytes 30917152 | solution.py:161
  84.7 6.4 %conditional.4 = ((f32[4,1024]{1,0:T(4,128)S(1)}, f32[4,1024]{1,0:T(4,128)S(1)}, f32[1024,4,64]{0,2,1:T(8,128)S(1)})) conditional(s32[]{:T(128)} %clamp.12, (f32[4,1024]{1,0:T(4,128)S(1)}, f32[4,1024]{1,0:T(4,128)S(1)}, f32[1024,4,64]{0,2,1:T(8,128)S(1)}) %tuple.75, (bf16[512,64]{0,1:T(8,128)(2,1)S(1)}, ...), branch_computations={%region_4.4_spmd, %region_5.7_spmd, %region_8.10_spmd} | conditional | flops 577779200 | bytes 30369832 | solution.py:158
  93.8 6.4 %conditional.4 = ((f32[4,1024]{1,0:T(4,128)S(1)}, f32[4,1024]{1,0:T(4,128)S(1)}, f32[1024,4,64]{0,2,1:T(8,128)S(1)})) conditional(s32[]{:T(128)} %clamp.12, (f32[4,1024]{1,0:T(4,128)S(1)}, f32[4,1024]{1,0:T(4,128)S(1)}, f32[1024,4,64]{0,2,1:T(8,128)S(1)}) %tuple.75, (bf16[512,64]{0,1:T(8,128)(2,1)S(1)}, ...), branch_computations={%region_4.4_spmd, %region_5.7_spmd, %region_8.10_spmd} | conditional | flops 577779200 | bytes 30369832 | solution.py:158
  95.4 2.7 %fusion.11 = f32[1024,4,64]{0,2,1:T(8,128)S(1)} fusion(f32[512,1024,4]{1,0,2:T(8,128)S(1)} %get-tuple-element.449, f32[4,1024]{1,0:T(4,128)S(1)} %get-tuple-element.542, f32[4,512]{1,0:T(4,128)S(1)} %get-tuple-element.292, f32[4,1024]{1,0:T(4,128)S(1)} %get-tuple-element.291, f32[1024,4,64]{0,2,1:T(8,128)S(1)} %get-tuple-element.294, ...), kind=kOutput, calls=%fused_computation.9 | convolution fusion | flops 279445504 | bytes 10608640 | tf_op jit(solution)/shard_map/while/body/eval_jaxpr/cond/branch_1_fun/htu,ud->thd/dot_general | solution.py:50
  102.8 6.4 %conditional.4 = ((f32[4,1024]{1,0:T(4,128)S(1)}, f32[4,1024]{1,0:T(4,128)S(1)}, f32[1024,4,64]{0,2,1:T(8,128)S(1)})) conditional(s32[]{:T(128)} %clamp.12, (f32[4,1024]{1,0:T(4,128)S(1)}, f32[4,1024]{1,0:T(4,128)S(1)}, f32[1024,4,64]{0,2,1:T(8,128)S(1)}) %tuple.75, (bf16[512,64]{0,1:T(8,128)(2,1)S(1)}, ...), branch_computations={%region_4.4_spmd, %region_5.7_spmd, %region_8.10_spmd} | conditional | flops 577779200 | bytes 30369832 | solution.py:158
  111.9 6.4 %conditional.4 = ((f32[4,1024]{1,0:T(4,128)S(1)}, f32[4,1024]{1,0:T(4,128)S(1)}, f32[1024,4,64]{0,2,1:T(8,128)S(1)})) conditional(s32[]{:T(128)} %clamp.12, (f32[4,1024]{1,0:T(4,128)S(1)}, f32[4,1024]{1,0:T(4,128)S(1)}, f32[1024,4,64]{0,2,1:T(8,128)S(1)}) %tuple.75, (bf16[512,64]{0,1:T(8,128)(2,1)S(1)}, ...), branch_computations={%region_4.4_spmd, %region_5.7_spmd, %region_8.10_spmd} | conditional | flops 577779200 | bytes 30369832 | solution.py:158
  113.5 2.7 %fusion.11 = f32[1024,4,64]{0,2,1:T(8,128)S(1)} fusion(f32[512,1024,4]{1,0,2:T(8,128)S(1)} %get-tuple-element.449, f32[4,1024]{1,0:T(4,128)S(1)} %get-tuple-element.542, f32[4,512]{1,0:T(4,128)S(1)} %get-tuple-element.292, f32[4,1024]{1,0:T(4,128)S(1)} %get-tuple-element.291, f32[1024,4,64]{0,2,1:T(8,128)S(1)} %get-tuple-element.294, ...), kind=kOutput, calls=%fused_computation.9 | convolution fusion | flops 279445504 | bytes 10608640 | tf_op jit(solution)/shard_map/while/body/eval_jaxpr/cond/branch_1_fun/htu,ud->thd/dot_general | solution.py:50
  121.0 6.4 %conditional.4 = ((f32[4,1024]{1,0:T(4,128)S(1)}, f32[4,1024]{1,0:T(4,128)S(1)}, f32[1024,4,64]{0,2,1:T(8,128)S(1)})) conditional(s32[]{:T(128)} %clamp.12, (f32[4,1024]{1,0:T(4,128)S(1)}, f32[4,1024]{1,0:T(4,128)S(1)}, f32[1024,4,64]{0,2,1:T(8,128)S(1)}) %tuple.75, (bf16[512,64]{0,1:T(8,128)(2,1)S(1)}, ...), branch_computations={%region_4.4_spmd, %region_5.7_spmd, %region_8.10_spmd} | conditional | flops 577779200 | bytes 30369832 | solution.py:158
  130.1 6.4 %conditional.4 = ((f32[4,1024]{1,0:T(4,128)S(1)}, f32[4,1024]{1,0:T(4,128)S(1)}, f32[1024,4,64]{0,2,1:T(8,128)S(1)})) conditional(s32[]{:T(128)} %clamp.12, (f32[4,1024]{1,0:T(4,128)S(1)}, f32[4,1024]{1,0:T(4,128)S(1)}, f32[1024,4,64]{0,2,1:T(8,128)S(1)}) %tuple.75, (bf16[512,64]{0,1:T(8,128)(2,1)S(1)}, ...), branch_computations={%region_4.4_spmd, %region_5.7_spmd, %region_8.10_spmd} | conditional | flops 577779200 | bytes 30369832 | solution.py:158
  131.7 2.7 %fusion.11 = f32[1024,4,64]{0,2,1:T(8,128)S(1)} fusion(f32[512,1024,4]{1,0,2:T(8,128)S(1)} %get-tuple-element.449, f32[4,1024]{1,0:T(4,128)S(1)} %get-tuple-element.542, f32[4,512]{1,0:T(4,128)S(1)} %get-tuple-element.292, f32[4,1024]{1,0:T(4,128)S(1)} %get-tuple-element.291, f32[1024,4,64]{0,2,1:T(8,128)S(1)} %get-tuple-element.294, ...), kind=kOutput, calls=%fused_computation.9 | convolution fusion | flops 279445504 | bytes 10608640 | tf_op jit(solution)/shard_map/while/body/eval_jaxpr/cond/branch_1_fun/htu,ud->thd/dot_general | solution.py:50
  139.1 6.4 %conditional.4 = ((f32[4,1024]{1,0:T(4,128)S(1)}, f32[4,1024]{1,0:T(4,128)S(1)}, f32[1024,4,64]{0,2,1:T(8,128)S(1)})) conditional(s32[]{:T(128)} %clamp.12, (f32[4,1024]{1,0:T(4,128)S(1)}, f32[4,1024]{1,0:T(4,128)S(1)}, f32[1024,4,64]{0,2,1:T(8,128)S(1)}) %tuple.75, (bf16[512,64]{0,1:T(8,128)(2,1)S(1)}, ...), branch_computations={%region_4.4_spmd, %region_5.7_spmd, %region_8.10_spmd} | conditional | flops 577779200 | bytes 30369832 | solution.py:158
  148.2 6.4 %conditional.4 = ((f32[4,1024]{1,0:T(4,128)S(1)}, f32[4,1024]{1,0:T(4,128)S(1)}, f32[1024,4,64]{0,2,1:T(8,128)S(1)})) conditional(s32[]{:T(128)} %clamp.12, (f32[4,1024]{1,0:T(4,128)S(1)}, f32[4,1024]{1,0:T(4,128)S(1)}, f32[1024,4,64]{0,2,1:T(8,128)S(1)}) %tuple.75, (bf16[512,64]{0,1:T(8,128)(2,1)S(1)}, ...), branch_computations={%region_4.4_spmd, %region_5.7_spmd, %region_8.10_spmd} | conditional | flops 577779200 | bytes 30369832 | solution.py:158
  157.3 6.4 %conditional.4 = ((f32[4,1024]{1,0:T(4,128)S(1)}, f32[4,1024]{1,0:T(4,128)S(1)}, f32[1024,4,64]{0,2,1:T(8,128)S(1)})) conditional(s32[]{:T(128)} %clamp.12, (f32[4,1024]{1,0:T(4,128)S(1)}, f32[4,1024]{1,0:T(4,128)S(1)}, f32[1024,4,64]{0,2,1:T(8,128)S(1)}) %tuple.75, (bf16[512,64]{0,1:T(8,128)(2,1)S(1)}, ...), branch_computations={%region_4.4_spmd, %region_5.7_spmd, %region_8.10_spmd} | conditional | flops 577779200 | bytes 30369832 | solution.py:158
  166.4 6.4 %conditional.4 = ((f32[4,1024]{1,0:T(4,128)S(1)}, f32[4,1024]{1,0:T(4,128)S(1)}, f32[1024,4,64]{0,2,1:T(8,128)S(1)})) conditional(s32[]{:T(128)} %clamp.12, (f32[4,1024]{1,0:T(4,128)S(1)}, f32[4,1024]{1,0:T(4,128)S(1)}, f32[1024,4,64]{0,2,1:T(8,128)S(1)}) %tuple.75, (bf16[512,64]{0,1:T(8,128)(2,1)S(1)}, ...), branch_computations={%region_4.4_spmd, %region_5.7_spmd, %region_8.10_spmd} | conditional | flops 577779200 | bytes 30369832 | solution.py:158
  168.0 2.7 %fusion.11 = f32[1024,4,64]{0,2,1:T(8,128)S(1)} fusion(f32[512,1024,4]{1,0,2:T(8,128)S(1)} %get-tuple-element.449, f32[4,1024]{1,0:T(4,128)S(1)} %get-tuple-element.542, f32[4,512]{1,0:T(4,128)S(1)} %get-tuple-element.292, f32[4,1024]{1,0:T(4,128)S(1)} %get-tuple-element.291, f32[1024,4,64]{0,2,1:T(8,128)S(1)} %get-tuple-element.294, ...), kind=kOutput, calls=%fused_computation.9 | convolution fusion | flops 279445504 | bytes 10608640 | tf_op jit(solution)/shard_map/while/body/eval_jaxpr/cond/branch_1_fun/htu,ud->thd/dot_general | solution.py:50
  175.5 6.4 %conditional.4 = ((f32[4,1024]{1,0:T(4,128)S(1)}, f32[4,1024]{1,0:T(4,128)S(1)}, f32[1024,4,64]{0,2,1:T(8,128)S(1)})) conditional(s32[]{:T(128)} %clamp.12, (f32[4,1024]{1,0:T(4,128)S(1)}, f32[4,1024]{1,0:T(4,128)S(1)}, f32[1024,4,64]{0,2,1:T(8,128)S(1)}) %tuple.75, (bf16[512,64]{0,1:T(8,128)(2,1)S(1)}, ...), branch_computations={%region_4.4_spmd, %region_5.7_spmd, %region_8.10_spmd} | conditional | flops 577779200 | bytes 30369832 | solution.py:158
  184.5 6.4 %conditional.4 = ((f32[4,1024]{1,0:T(4,128)S(1)}, f32[4,1024]{1,0:T(4,128)S(1)}, f32[1024,4,64]{0,2,1:T(8,128)S(1)})) conditional(s32[]{:T(128)} %clamp.12, (f32[4,1024]{1,0:T(4,128)S(1)}, f32[4,1024]{1,0:T(4,128)S(1)}, f32[1024,4,64]{0,2,1:T(8,128)S(1)}) %tuple.75, (bf16[512,64]{0,1:T(8,128)(2,1)S(1)}, ...), branch_computations={%region_4.4_spmd, %region_5.7_spmd, %region_8.10_spmd} | conditional | flops 577779200 | bytes 30369832 | solution.py:158
  193.6 6.4 %conditional.4 = ((f32[4,1024]{1,0:T(4,128)S(1)}, f32[4,1024]{1,0:T(4,128)S(1)}, f32[1024,4,64]{0,2,1:T(8,128)S(1)})) conditional(s32[]{:T(128)} %clamp.12, (f32[4,1024]{1,0:T(4,128)S(1)}, f32[4,1024]{1,0:T(4,128)S(1)}, f32[1024,4,64]{0,2,1:T(8,128)S(1)}) %tuple.75, (bf16[512,64]{0,1:T(8,128)(2,1)S(1)}, ...), branch_computations={%region_4.4_spmd, %region_5.7_spmd, %region_8.10_spmd} | conditional | flops 577779200 | bytes 30369832 | solution.py:158
  202.7 6.4 %conditional.4 = ((f32[4,1024]{1,0:T(4,128)S(1)}, f32[4,1024]{1,0:T(4,128)S(1)}, f32[1024,4,64]{0,2,1:T(8,128)S(1)})) conditional(s32[]{:T(128)} %clamp.12, (f32[4,1024]{1,0:T(4,128)S(1)}, f32[4,1024]{1,0:T(4,128)S(1)}, f32[1024,4,64]{0,2,1:T(8,128)S(1)}) %tuple.75, (bf16[512,64]{0,1:T(8,128)(2,1)S(1)}, ...), branch_computations={%region_4.4_spmd, %region_5.7_spmd, %region_8.10_spmd} | conditional | flops 577779200 | bytes 30369832 | solution.py:158
  204.3 2.7 %fusion.11 = f32[1024,4,64]{0,2,1:T(8,128)S(1)} fusion(f32[512,1024,4]{1,0,2:T(8,128)S(1)} %get-tuple-element.449, f32[4,1024]{1,0:T(4,128)S(1)} %get-tuple-element.542, f32[4,512]{1,0:T(4,128)S(1)} %get-tuple-element.292, f32[4,1024]{1,0:T(4,128)S(1)} %get-tuple-element.291, f32[1024,4,64]{0,2,1:T(8,128)S(1)} %get-tuple-element.294, ...), kind=kOutput, calls=%fused_computation.9 | convolution fusion | flops 279445504 | bytes 10608640 | tf_op jit(solution)/shard_map/while/body/eval_jaxpr/cond/branch_1_fun/htu,ud->thd/dot_general | solution.py:50
  211.8 9.4 %conditional.4 = ((f32[4,1024]{1,0:T(4,128)S(1)}, f32[4,1024]{1,0:T(4,128)S(1)}, f32[1024,4,64]{0,2,1:T(8,128)S(1)})) conditional(s32[]{:T(128)} %clamp.12, (f32[4,1024]{1,0:T(4,128)S(1)}, f32[4,1024]{1,0:T(4,128)S(1)}, f32[1024,4,64]{0,2,1:T(8,128)S(1)}) %tuple.75, (bf16[512,64]{0,1:T(8,128)(2,1)S(1)}, ...), branch_computations={%region_4.4_spmd, %region_5.7_spmd, %region_8.10_spmd} | conditional | flops 577779200 | bytes 30369832 | solution.py:158
  214.6 3.3 %fusion.30 = f32[1024,4,64]{0,2,1:T(8,128)S(1)} fusion(f32[512,1024,4]{1,0,2:T(8,128)S(1)} %get-tuple-element.451, f32[4,1024]{1,0:T(4,128)S(1)} %get-tuple-element.545, f32[4,512]{1,0:T(4,128)S(1)} %get-tuple-element.303, f32[4,1024]{1,0:T(4,128)S(1)} %get-tuple-element.302, pred[1024,512]{0,1:T(8,128)(4,1)S(1)} %broadcast_compare_fusion, ...), kind=kOutput, calls=%fused_computation.27 | convolution fusion | flops 283639808 | bytes 11132928 | tf_op jit(solution)/shard_map/while/body/eval_jaxpr/cond/branch_2_fun/htu,ud->thd/dot_general | solution.py:50
  217.9 3.2 %fusion.22 = f32[4,1024]{1,0:T(4,128)S(1)} fusion(f32[512,1024,4]{1,0,2:T(8,128)S(1)} %get-tuple-element.451, f32[4,1024]{1,0:T(4,128)S(1)} %get-tuple-element.545, f32[4,512]{1,0:T(4,128)S(1)} %get-tuple-element.303, f32[4,1024]{1,0:T(4,128)S(1)} %get-tuple-element.302, pred[1024,512]{0,1:T(8,128)(4,1)S(1)} %broadcast_compare_fusion), kind=kLoop, calls=%fused_computation.22 | loop fusion | flops 14675968 | bytes 8970240 | tf_op jit(solution)/shard_map/while/body/eval_jaxpr/cond/branch_2_fun/reduce_sum | solution.py:49
  223.8 9.4 %conditional.4 = ((f32[4,1024]{1,0:T(4,128)S(1)}, f32[4,1024]{1,0:T(4,128)S(1)}, f32[1024,4,64]{0,2,1:T(8,128)S(1)})) conditional(s32[]{:T(128)} %clamp.12, (f32[4,1024]{1,0:T(4,128)S(1)}, f32[4,1024]{1,0:T(4,128)S(1)}, f32[1024,4,64]{0,2,1:T(8,128)S(1)}) %tuple.75, (bf16[512,64]{0,1:T(8,128)(2,1)S(1)}, ...), branch_computations={%region_4.4_spmd, %region_5.7_spmd, %region_8.10_spmd} | conditional | flops 577779200 | bytes 30369832 | solution.py:158
  226.6 3.3 %fusion.30 = f32[1024,4,64]{0,2,1:T(8,128)S(1)} fusion(f32[512,1024,4]{1,0,2:T(8,128)S(1)} %get-tuple-element.451, f32[4,1024]{1,0:T(4,128)S(1)} %get-tuple-element.545, f32[4,512]{1,0:T(4,128)S(1)} %get-tuple-element.303, f32[4,1024]{1,0:T(4,128)S(1)} %get-tuple-element.302, pred[1024,512]{0,1:T(8,128)(4,1)S(1)} %broadcast_compare_fusion, ...), kind=kOutput, calls=%fused_computation.27 | convolution fusion | flops 283639808 | bytes 11132928 | tf_op jit(solution)/shard_map/while/body/eval_jaxpr/cond/branch_2_fun/htu,ud->thd/dot_general | solution.py:50
  230.0 3.2 %fusion.22 = f32[4,1024]{1,0:T(4,128)S(1)} fusion(f32[512,1024,4]{1,0,2:T(8,128)S(1)} %get-tuple-element.451, f32[4,1024]{1,0:T(4,128)S(1)} %get-tuple-element.545, f32[4,512]{1,0:T(4,128)S(1)} %get-tuple-element.303, f32[4,1024]{1,0:T(4,128)S(1)} %get-tuple-element.302, pred[1024,512]{0,1:T(8,128)(4,1)S(1)} %broadcast_compare_fusion), kind=kLoop, calls=%fused_computation.22 | loop fusion | flops 14675968 | bytes 8970240 | tf_op jit(solution)/shard_map/while/body/eval_jaxpr/cond/branch_2_fun/reduce_sum | solution.py:49
  233.8 11.3 %all_to_all.25 = bf16[4,256,256]{1,2,0:T(8,128)(2,1)S(1)} all-to-all(bf16[4,256,256]{1,2,0:T(8,128)(2,1)S(1)} %copy.52), channel_id=1, replica_groups=mesh['sp'=8,'tp'=4] {'tp'}, dimensions={0} | all-to-all | bytes 1048576 | tf_op jit(solution)/shard_map/all_to_all | solution.py:166
  245.1 4.4 %convolution_convert_fusion = bf16[256,2048]{1,0:T(8,128)(2,1)} fusion(bf16[256,1024]{0,1:T(8,128)(2,1)S(1)} %bitcast.114, bf16[1024,2048]{1,0:T(8,128)(2,1)} %param.22), kind=kOutput, calls=%fused_computation.44 | convolution fusion | flops 1074266112 | bytes 5767168 | tf_op jit(solution)/shard_map/dot_general | solution.py:167
  (245 shorter events, 121.8 us)
Async XLA Ops:
  6.5 1.6 copy-start
  6.5 75.4 %all-gather.2.cloned.1.call-start = ((), (), s32[]{:S(2)}) async-start(), calls=%async_computation.2 | async-start | bytes 2359296 | tf_op jit(solution)/shard_map/all_gather | solution.py:118
  8.1 10.6 %copy-start.3 = (f32[64]{0:T(128)S(1)}, f32[64]{0:T(128)}, u32[]{:S(2)}) copy-start(f32[64]{0:T(128)} %param.19) | copy-start | bytes 772
  8.1 10.7 %copy-start.2 = (f32[64]{0:T(128)S(1)}, f32[64]{0:T(128)}, u32[]{:S(2)}) copy-start(f32[64]{0:T(128)} %param.20) | copy-start | bytes 772
  16.7 18.0 %copy-start.1 = (f32[1024,4]{0,1:T(4,128)S(1)}, f32[1024,4]{0,1:T(4,128)}, u32[]{:S(2)}) copy-start(f32[1024,4]{0,1:T(4,128)} %param.21) | copy-start | bytes 49156
Sparse Core Ops, SparseCore 0:
  34.9 46.9 all-gather.1
